TPU v7x, 32 devices: a whole 2x2x4 slice. The times are simulated.
32 devices in a mesh: ep: 8 (over z, core), tp: 4 (over y, x).
Axes of the slice: x: 2, y: 2, z: 4, core: 2. Of those that a mesh axis runs over, the one named last changes fastest.
Arguments:
- attn_in: bfloat16 [4096, 2048], P('ep'), may hold values from -6 to 6
- mix_gain: float32 [2048], replicated, may hold values from 0.1 to 1.9
- query_weight: bfloat16 [2048, 1024], P(None, 'tp'), may hold values from -0.125 to 0.125
- key_weight: bfloat16 [2048, 1024], P(None, 'tp'), may hold values from -0.125 to 0.125
- value_weight: bfloat16 [2048, 1024], P(None, 'tp'), may hold values from -0.125 to 0.125
- query_gain: float32 [64], replicated, may hold values from 0.7 to 6
- key_gain: float32 [64], replicated, may hold values from 0.7 to 6
- log_cache: float32 [4096, 16], P('ep', 'tp'), as said below
- head_gain: float32 [1024], P('tp'), may hold values from 0.1 to 1.9
- out_weight: bfloat16 [1024, 2048], P(None, 'tp'), may hold values from -0.1875 to 0.1875
- moe_in: bfloat16 [1024, 2048], P('ep'), may hold values from -6 to 6
- moe_gain: float32 [2048], replicated, may hold values from 0.1 to 1.9
- routes: int32 [1024, 2], P('ep'), may hold values from 0 to 7, all different within a row; in each aligned block of 128 rows (0 to 127, 128 to 255, ...) at most 48 rows name the same one
- route_weight: float32 [1024, 2], P('ep'), may hold values from 0.25 to 1
- expert_gate: bfloat16 [8, 2048, 1024], P('ep', None, 'tp'), may hold values from -0.125 to 0.125
- expert_up: bfloat16 [8, 2048, 1024], P('ep', None, 'tp'), may hold values from -0.125 to 0.125
- expert_down: bfloat16 [8, 1024, 2048], P('ep', 'tp'), may hold values from -0.1875 to 0.1875
Outputs:
- mixer_out: bfloat16 [4096, 2048], P('ep', 'tp')
- moe_out: bfloat16 [1024, 2048], P('ep', 'tp')
Inputs may be any that keep to these rules, and one draw needn't show every extreme that they name: `routes`: each row names 2 different experts; within the rows of one index of ep (aligned blocks of 128 rows) no expert is named by more than 48 rows. `log_cache`: never increasing along positions for each head.
All inputs are finite; a program needn't handle non-finite values.
Results may differ from a plain program's by a relative error of at most 0.015.
The roundings to bfloat16 on the way count: a program that leaves them out, or rounds other values in their place, can miss the bound.
Values may be sent and summed in bfloat16 or wider, within the bound.
A program may use at most 64 MiB of HBM per device.

v0:
```python
import math
import jax
import jax.numpy as jnp
from jax import lax
from jax.sharding import PartitionSpec as P

HD = 64
epsilon = 1e-06


def row_norm(inputs, gain_vec):
    floats = inputs.astype(jnp.float32)
    scaled = floats * lax.rsqrt(jnp.mean(floats * floats, axis=-1, keepdims=True) + epsilon)
    return scaled * gain_vec


def body(
    attn_in,
    mix_gain,
    query_weight,
    key_weight,
    value_weight,
    query_gain,
    key_gain,
    log_cache,
    head_gain,
    out_weight,
    moe_in,
    moe_gain,
    routes,
    route_weight,
    expert_gate,
    expert_up,
    expert_down,
):
    tok_rows = attn_in.shape[0]
    local_heads = query_weight.shape[1] // HD
    normed = row_norm(attn_in, mix_gain).astype(jnp.bfloat16)

    def project(weight):
        return jnp.dot(normed, weight, preferred_element_type=jnp.float32).reshape(
            tok_rows, local_heads, HD
        )

    queries = row_norm(project(query_weight), query_gain).astype(jnp.bfloat16)
    key_rows = (
        row_norm(project(key_weight), key_gain)
        .astype(jnp.bfloat16)
        .reshape(tok_rows, local_heads * HD)
    )
    value_rows = project(value_weight).astype(jnp.bfloat16).reshape(tok_rows, local_heads * HD)
    all_gates = lax.all_gather(log_cache, "ep", axis=0, tiled=True)
    query_pos = lax.axis_index("ep") * tok_rows + jnp.arange(tok_rows, dtype=jnp.int32)
    query_gates = jnp.transpose(log_cache)[:, :, None]
    score_scale = HD ** (-0.5)
    init_state = (
        jnp.full((local_heads, tok_rows), -1e30, jnp.float32),
        jnp.zeros((local_heads, tok_rows), jnp.float32),
        jnp.zeros((local_heads, tok_rows, HD), jnp.float32),
    )
    key_piece = lax.all_gather(key_rows, "ep", axis=0, tiled=True)
    value_piece = lax.all_gather(value_rows, "ep", axis=0, tiled=True)
    span_len = key_piece.shape[0]
    block_len = math.gcd(span_len, 512)

    def block_step(block_index, running):
        running_max, running_sum, weighted = running
        block_begin = block_index * block_len
        key_block = lax.dynamic_slice_in_dim(key_piece, block_begin, block_len, 0).reshape(
            block_len, local_heads, HD
        )
        value_block = lax.dynamic_slice_in_dim(value_piece, block_begin, block_len, 0).reshape(
            block_len, local_heads, HD
        )
        gate_block = lax.dynamic_slice_in_dim(all_gates, block_begin, block_len, 0)
        scores = (
            jnp.einsum("qhd,khd->hqk", queries, key_block, preferred_element_type=jnp.float32)
            * score_scale
        )
        scores = scores + query_gates - jnp.transpose(gate_block)[:, None, :]
        key_pos = block_begin + jnp.arange(block_len, dtype=jnp.int32)
        causal = (key_pos[None, :] <= query_pos[:, None])[None]
        new_max = jnp.maximum(running_max, jnp.max(jnp.where(causal, scores, -1e30), axis=2))
        expo_scores = jnp.where(causal, jnp.exp(scores - new_max[:, :, None]), 0.0)
        rescale = jnp.exp(running_max - new_max)
        running_sum = running_sum * rescale + jnp.sum(expo_scores, axis=2)
        weighted = weighted * rescale[:, :, None] + jnp.einsum(
            "hqk,khd->hqd",
            expo_scores.astype(jnp.bfloat16),
            value_block,
            preferred_element_type=jnp.float32,
        )
        return (new_max, running_sum, weighted)

    final_max, final_sum, weighted = lax.fori_loop(0, span_len // block_len, block_step, init_state)
    attended = jnp.transpose(weighted / final_sum[:, :, None], (1, 0, 2))
    head_out = (
        row_norm(attended, head_gain.reshape(local_heads, HD))
        .astype(jnp.bfloat16)
        .reshape(tok_rows, local_heads * HD)
    )
    mixer_out = jnp.dot(
        lax.all_gather(head_out, "tp", axis=1, tiled=True),
        out_weight,
        preferred_element_type=jnp.float32,
    ).astype(jnp.bfloat16)
    moe_rows = moe_in.shape[0]
    top_count = routes.shape[1]
    local_experts = expert_gate.shape[0]
    senders = lax.axis_size("ep")
    expert_count = local_experts * senders
    capacity = 3 * moe_rows * top_count // (2 * expert_count)
    model_width = moe_in.shape[1]
    moe_normed = row_norm(moe_in, moe_gain).astype(jnp.bfloat16)
    flat_routes = routes.reshape(-1)
    one_hot = (flat_routes[:, None] == jnp.arange(expert_count, dtype=jnp.int32)[None, :]).astype(
        jnp.int32
    )
    order_in = jnp.sum(jnp.cumsum(one_hot, axis=0) * one_hot, axis=1) - 1
    slot_index = flat_routes * capacity + order_in
    token_of = jnp.arange(flat_routes.shape[0], dtype=jnp.int32) // top_count
    source_row = jnp.zeros((expert_count * capacity,), jnp.int32).at[slot_index].set(token_of)
    filled = jnp.zeros((expert_count * capacity,), jnp.bool_).at[slot_index].set(True)
    send_buffer = jnp.where(
        filled[:, None], moe_normed[source_row], jnp.zeros((), jnp.bfloat16)
    ).reshape(expert_count, capacity, model_width)
    share_width = model_width // lax.axis_size("tp")
    share_part = lax.dynamic_slice_in_dim(
        send_buffer, lax.axis_index("tp") * share_width, share_width, 2
    )
    arrived = lax.all_to_all(share_part, "ep", split_axis=0, concat_axis=0, tiled=True)
    piece_now = lax.all_gather(arrived, "tp", axis=2, tiled=True)
    piece_cols = piece_now.shape[2]
    piece_rows = piece_now.reshape(senders, local_experts, capacity, piece_cols)
    gate_next = jnp.einsum(
        "sjcd,jdf->sjcf", piece_rows, expert_gate, preferred_element_type=jnp.float32
    )
    up_next = jnp.einsum(
        "sjcd,jdf->sjcf", piece_rows, expert_up, preferred_element_type=jnp.float32
    )
    hidden = (jax.nn.silu(gate_next) * up_next).astype(jnp.bfloat16)
    partial_value = jnp.einsum(
        "sjcf,jfd->sjcd", hidden, expert_down, preferred_element_type=jnp.float32
    )
    summed = lax.psum_scatter(
        partial_value.astype(jnp.bfloat16), "tp", scatter_dimension=3, tiled=True
    )
    out_cols = summed.shape[3]
    returned = lax.all_to_all(
        summed.reshape(expert_count, capacity, out_cols),
        "ep",
        split_axis=0,
        concat_axis=0,
        tiled=True,
    )
    picked = returned.reshape(expert_count * capacity, out_cols)[slot_index].astype(jnp.float32)
    weighted_rows = picked * route_weight.reshape(-1)[:, None]
    moe_out = jnp.sum(weighted_rows.reshape(moe_rows, top_count, out_cols), axis=1).astype(
        jnp.bfloat16
    )
    return (mixer_out, moe_out)


def solution(mesh):
    in_specs = (
        P("ep", None),
        P(),
        P(None, "tp"),
        P(None, "tp"),
        P(None, "tp"),
        P(),
        P(),
        P("ep", "tp"),
        P("tp"),
        P(None, "tp"),
        P("ep", None),
        P(),
        P("ep", None),
        P("ep", None),
        P("ep", None, "tp"),
        P("ep", None, "tp"),
        P("ep", "tp", None),
    )
    out_specs = (P("ep", "tp"), P("ep", "tp"))
    return jax.shard_map(body, mesh=mesh, in_specs=in_specs, out_specs=out_specs, check_vma=False)
```

profile of v0, /device:TPU:0, one launch (start us, length us, event | category | flops | bytes accessed | tf_op | source)
XLA Modules:
  0.0 263.2 jit_solution(7645723227461239029)
XLA Ops:
  10.3 1.4 scatter_custom_fusion.1
  11.7 1.2 fusion.23
  13.0 1.5 scatter_custom_fusion
  14.5 1.2 fusion.25
  15.8 2.5 gather_fusion
  18.4 18.8 %all_to_all.10 = bf16[8,48,512]{2,1,0:T(8,128)(2,1)} all-to-all(bf16[8,48,512]{2,1,0:T(8,128)(2,1)S(1)} %dynamic-slice_select_fusion), channel_id=1, replica_groups=mesh['ep'=8,'tp'=4] {'ep'}, dimensions={0} | all-to-all | bytes 786432 | tf_op jit(solution)/shard_map/all_to_all | solution.py:131
  37.4 2.2 fusion.16
  39.6 2.8 %bitcast_reduce_fusion = (f32[512,4]{0,1:T(4,128)S(1)}, f32[512,256]{0,1:T(8,128)S(1)}) fusion(bf16[2048,256]{1,0:T(8,128)(2,1)} %param.22, bf16[512,2048]{1,0:T(8,128)(2,1)} %param.19, f32[2048]{0:T(1024)S(1)} %copy-done.8, f32[512]{0:T(512)S(1)} %add_rsqrt_fusion.3), kind=kOutput, calls=%fused_computation.59 | convolution fusion | flops 541325312 | bytes 3688448 | tf_op jit(solution)/shard_map/dot_general | solution.py:41
  43.4 2.7 %convolution_convert_fusion.2 = bf16[512,256]{1,0:T(8,128)(2,1)} fusion(bf16[2048,256]{1,0:T(8,128)(2,1)} %param.23, bf16[512,2048]{1,0:T(8,128)(2,1)S(1)} %copy-done.1, f32[2048]{0:T(1024)S(1)} %copy-done.8, f32[512]{0:T(512)S(1)} %add_rsqrt_fusion.3), kind=kOutput, calls=%fused_computation.42 | convolution fusion | flops 541196288 | bytes 3418112 | tf_op jit(solution)/shard_map/dot_general | solution.py:41
  46.3 14.0 %all_gather.16 = f32[4096,4]{0,1:T(4,128)S(1)} all-gather(f32[512,4]{0,1:T(4,128)S(1)} %copy-done.3), channel_id=1, replica_groups=mesh['ep'=8,'tp'=4] {'ep'}, dimensions={0}, use_global_device_ids=true | all-gather | bytes 73728 | tf_op jit(solution)/shard_map/all_gather | solution.py:52
  60.2 2.2 multiply_reduce_fusion.1
  62.5 4.5 %all-gather.11.cloned.1.call-done = bf16[8,48,2048]{2,1,0:T(8,128)(2,1)} async-done(((bf16[8,48,512]{2,1,0:T(8,128)(2,1)}), bf16[8,48,2048]{2,1,0:T(8,128)(2,1)}) %all-gather.11.cloned.1.call-update) | async-done | bytes 1572880 | tf_op jit(solution)/shard_map/all_gather | solution.py:132
  67.0 2.3 convolution_bitcast_fusion.1
  69.3 4.8 %fusion.19 = bf16[8,1,48,2048]{3,2,0,1:T(8,128)(2,1)} fusion(bf16[1,256,2048]{2,1,0:T(8,128)(2,1)S(1)} %copy-done, bf16[8,48,2048]{2,1,0:T(8,128)(2,1)} %all-gather.11.cloned.1.call-done, bf16[1,2048,256]{2,1,0:T(8,128)(2,1)} %param.34, f32[8,1,48,256]{3,2,0,1:T(8,128)S(1)} %convolution_bitcast_fusion.1), kind=kOutput, calls=%fused_computation.35 | convolution fusion | flops 806682624 | bytes 5636096 | tf_op jit(solution)/shard_map/sjcf,jfd->sjcd/dot_general | solution.py:142
  74.4 23.4 %all-gather.5.cloned.1.call-done = bf16[4096,256]{0,1:T(8,128)(2,1)} async-done(((bf16[512,256]{0,1:T(8,128)(2,1)}), bf16[4096,256]{0,1:T(8,128)(2,1)}) %all-gather.5.cloned.1.call-update) | async-done | bytes 2097168 | tf_op jit(solution)/shard_map/all_gather | solution.py:61
  97.8 30.2 %all-gather.7.cloned.1.call-done = bf16[4096,256]{1,0:T(8,128)(2,1)} async-done(((bf16[512,256]{1,0:T(8,128)(2,1)}), bf16[4096,256]{1,0:T(8,128)(2,1)}) %all-gather.7.cloned.1.call-update) | async-done | bytes 2097168 | tf_op jit(solution)/shard_map/all_gather | solution.py:62
  128.0 95.6 %while.18 = (s32[]{:T(128)}, f32[4,512]{1,0:T(4,128)S(1)}, f32[4,512]{1,0:T(4,128)S(1)}, f32[4,512,64]{1,2,0:T(8,128)S(1)}, bf16[4096,256]{0,1:T(8,128)(2,1)}, /...) while((s32[]{:T(128)}, f32[4,512]{1,0:T(4,128)S(1)}, ...), condition=%wide.region_6.7_spmd.clone, body=%wide.region_3.6_spmd.clone.sunk | while | flops 286927872 | bytes 17244372 | solution.py:95
  129.2 3.1 %fusion.76 = (f32[4,512]{1,0:T(4,128)S(1)}, f32[4,512,512]{2,1,0:T(8,128)}) fusion(f32[4,512]{1,0:T(4,128)S(1)} %dynamic-slice_bitcast_fusion.2, f32[4,512]{1,0:T(4,128)S(1)} %bitcast.137, pred[512,512]{0,1:T(8,128)(4,1)S(1)} %broadcast_compare_fusion.2, bf16[512,4,64]{0,2,1:T(8,128)(2,1)S(1)} %bitcast.131, ...), kind=kOutput, calls=%fused_computation.7.clone.1 | convolution fusion | flops 139458560 | bytes 5005312 | tf_op jit(solution)/shard_map/while/body/eval_jaxpr/qhd,khd->hqk/dot_general | solution.py:77
  132.3 2.9 %fusion.77 = f32[4,512]{1,0:T(4,128)S(1)} fusion(f32[4,512,512]{2,1,0:T(8,128)} %get-tuple-element.330, f32[4,512]{1,0:T(4,128)S(1)} %select_maximum_fusion.2, f32[4,512]{1,0:T(4,128)S(1)} %dynamic-slice_bitcast_fusion.2, f32[4,512]{1,0:T(4,128)S(1)} %bitcast.138, pred[512,512]{0,1:T(8,128)(4,1)S(1)} %broadcast_compare_fusion.2), kind=kLoop, calls=%fused_computation.12.clone.1 | loop fusion | flops 6289408 | bytes 4489216 | tf_op jit(solution)/shard_map/while/body/eval_jaxpr/reduce_sum | solution.py:86
  136.4 3.5 %fusion.79 = f32[4,512,64]{1,2,0:T(8,128)S(1)} fusion(bf16[512,4,64]{0,2,1:T(8,128)(2,1)S(1)} %bitcast.132, f32[4,512,512]{2,1,0:T(8,128)} %get-tuple-element.330, f32[4,512]{1,0:T(4,128)S(1)} %select_maximum_fusion.2, f32[4,512]{1,0:T(4,128)S(1)} %dynamic-slice_bitcast_fusion.2, f32[4,512]{1,0:T(4,128)S(1)} %bitcast.139, ...), kind=kOutput, calls=%fused_computation.15.clone.1 | convolution fusion | flops 140902400 | bytes 5799937 | tf_op jit(solution)/shard_map/while/body/eval_jaxpr/hqk,khd->hqd/dot_general | solution.py:87
  141.2 3.1 %fusion.76 = (f32[4,512]{1,0:T(4,128)S(1)}, f32[4,512,512]{2,1,0:T(8,128)}) fusion(f32[4,512]{1,0:T(4,128)S(1)} %dynamic-slice_bitcast_fusion.2, f32[4,512]{1,0:T(4,128)S(1)} %bitcast.137, pred[512,512]{0,1:T(8,128)(4,1)S(1)} %broadcast_compare_fusion.2, bf16[512,4,64]{0,2,1:T(8,128)(2,1)S(1)} %bitcast.131, ...), kind=kOutput, calls=%fused_computation.7.clone.1 | convolution fusion | flops 139458560 | bytes 5005312 | tf_op jit(solution)/shard_map/while/body/eval_jaxpr/qhd,khd->hqk/dot_general | solution.py:77
  144.3 3.0 %fusion.77 = f32[4,512]{1,0:T(4,128)S(1)} fusion(f32[4,512,512]{2,1,0:T(8,128)} %get-tuple-element.330, f32[4,512]{1,0:T(4,128)S(1)} %select_maximum_fusion.2, f32[4,512]{1,0:T(4,128)S(1)} %dynamic-slice_bitcast_fusion.2, f32[4,512]{1,0:T(4,128)S(1)} %bitcast.138, pred[512,512]{0,1:T(8,128)(4,1)S(1)} %broadcast_compare_fusion.2), kind=kLoop, calls=%fused_computation.12.clone.1 | loop fusion | flops 6289408 | bytes 4489216 | tf_op jit(solution)/shard_map/while/body/eval_jaxpr/reduce_sum | solution.py:86
  147.3 1.0 constant_dynamic-slice_fusion.5
  148.4 3.5 %fusion.79 = f32[4,512,64]{1,2,0:T(8,128)S(1)} fusion(bf16[512,4,64]{0,2,1:T(8,128)(2,1)S(1)} %bitcast.132, f32[4,512,512]{2,1,0:T(8,128)} %get-tuple-element.330, f32[4,512]{1,0:T(4,128)S(1)} %select_maximum_fusion.2, f32[4,512]{1,0:T(4,128)S(1)} %dynamic-slice_bitcast_fusion.2, f32[4,512]{1,0:T(4,128)S(1)} %bitcast.139, ...), kind=kOutput, calls=%fused_computation.15.clone.1 | convolution fusion | flops 140902400 | bytes 5799937 | tf_op jit(solution)/shard_map/while/body/eval_jaxpr/hqk,khd->hqd/dot_general | solution.py:87
  153.2 3.1 %fusion.76 = (f32[4,512]{1,0:T(4,128)S(1)}, f32[4,512,512]{2,1,0:T(8,128)}) fusion(f32[4,512]{1,0:T(4,128)S(1)} %dynamic-slice_bitcast_fusion.2, f32[4,512]{1,0:T(4,128)S(1)} %bitcast.137, pred[512,512]{0,1:T(8,128)(4,1)S(1)} %broadcast_compare_fusion.2, bf16[512,4,64]{0,2,1:T(8,128)(2,1)S(1)} %bitcast.131, ...), kind=kOutput, calls=%fused_computation.7.clone.1 | convolution fusion | flops 139458560 | bytes 5005312 | tf_op jit(solution)/shard_map/while/body/eval_jaxpr/qhd,khd->hqk/dot_general | solution.py:77
  156.3 2.9 %fusion.77 = f32[4,512]{1,0:T(4,128)S(1)} fusion(f32[4,512,512]{2,1,0:T(8,128)} %get-tuple-element.330, f32[4,512]{1,0:T(4,128)S(1)} %select_maximum_fusion.2, f32[4,512]{1,0:T(4,128)S(1)} %dynamic-slice_bitcast_fusion.2, f32[4,512]{1,0:T(4,128)S(1)} %bitcast.138, pred[512,512]{0,1:T(8,128)(4,1)S(1)} %broadcast_compare_fusion.2), kind=kLoop, calls=%fused_computation.12.clone.1 | loop fusion | flops 6289408 | bytes 4489216 | tf_op jit(solution)/shard_map/while/body/eval_jaxpr/reduce_sum | solution.py:86
  159.2 1.0 constant_dynamic-slice_fusion.5
  160.4 3.6 %fusion.79 = f32[4,512,64]{1,2,0:T(8,128)S(1)} fusion(bf16[512,4,64]{0,2,1:T(8,128)(2,1)S(1)} %bitcast.132, f32[4,512,512]{2,1,0:T(8,128)} %get-tuple-element.330, f32[4,512]{1,0:T(4,128)S(1)} %select_maximum_fusion.2, f32[4,512]{1,0:T(4,128)S(1)} %dynamic-slice_bitcast_fusion.2, f32[4,512]{1,0:T(4,128)S(1)} %bitcast.139, ...), kind=kOutput, calls=%fused_computation.15.clone.1 | convolution fusion | flops 140902400 | bytes 5799937 | tf_op jit(solution)/shard_map/while/body/eval_jaxpr/hqk,khd->hqd/dot_general | solution.py:87
  165.2 3.1 %fusion.76 = (f32[4,512]{1,0:T(4,128)S(1)}, f32[4,512,512]{2,1,0:T(8,128)}) fusion(f32[4,512]{1,0:T(4,128)S(1)} %dynamic-slice_bitcast_fusion.2, f32[4,512]{1,0:T(4,128)S(1)} %bitcast.137, pred[512,512]{0,1:T(8,128)(4,1)S(1)} %broadcast_compare_fusion.2, bf16[512,4,64]{0,2,1:T(8,128)(2,1)S(1)} %bitcast.131, ...), kind=kOutput, calls=%fused_computation.7.clone.1 | convolution fusion | flops 139458560 | bytes 5005312 | tf_op jit(solution)/shard_map/while/body/eval_jaxpr/qhd,khd->hqk/dot_general | solution.py:77
  168.3 2.9 %fusion.77 = f32[4,512]{1,0:T(4,128)S(1)} fusion(f32[4,512,512]{2,1,0:T(8,128)} %get-tuple-element.330, f32[4,512]{1,0:T(4,128)S(1)} %select_maximum_fusion.2, f32[4,512]{1,0:T(4,128)S(1)} %dynamic-slice_bitcast_fusion.2, f32[4,512]{1,0:T(4,128)S(1)} %bitcast.138, pred[512,512]{0,1:T(8,128)(4,1)S(1)} %broadcast_compare_fusion.2), kind=kLoop, calls=%fused_computation.12.clone.1 | loop fusion | flops 6289408 | bytes 4489216 | tf_op jit(solution)/shard_map/while/body/eval_jaxpr/reduce_sum | solution.py:86
  172.3 3.5 %fusion.79 = f32[4,512,64]{1,2,0:T(8,128)S(1)} fusion(bf16[512,4,64]{0,2,1:T(8,128)(2,1)S(1)} %bitcast.132, f32[4,512,512]{2,1,0:T(8,128)} %get-tuple-element.330, f32[4,512]{1,0:T(4,128)S(1)} %select_maximum_fusion.2, f32[4,512]{1,0:T(4,128)S(1)} %dynamic-slice_bitcast_fusion.2, f32[4,512]{1,0:T(4,128)S(1)} %bitcast.139, ...), kind=kOutput, calls=%fused_computation.15.clone.1 | convolution fusion | flops 140902400 | bytes 5799937 | tf_op jit(solution)/shard_map/while/body/eval_jaxpr/hqk,khd->hqd/dot_general | solution.py:87
  177.1 3.1 %fusion.76 = (f32[4,512]{1,0:T(4,128)S(1)}, f32[4,512,512]{2,1,0:T(8,128)}) fusion(f32[4,512]{1,0:T(4,128)S(1)} %dynamic-slice_bitcast_fusion.2, f32[4,512]{1,0:T(4,128)S(1)} %bitcast.137, pred[512,512]{0,1:T(8,128)(4,1)S(1)} %broadcast_compare_fusion.2, bf16[512,4,64]{0,2,1:T(8,128)(2,1)S(1)} %bitcast.131, ...), kind=kOutput, calls=%fused_computation.7.clone.1 | convolution fusion | flops 139458560 | bytes 5005312 | tf_op jit(solution)/shard_map/while/body/eval_jaxpr/qhd,khd->hqk/dot_general | solution.py:77
  180.2 2.9 %fusion.77 = f32[4,512]{1,0:T(4,128)S(1)} fusion(f32[4,512,512]{2,1,0:T(8,128)} %get-tuple-element.330, f32[4,512]{1,0:T(4,128)S(1)} %select_maximum_fusion.2, f32[4,512]{1,0:T(4,128)S(1)} %dynamic-slice_bitcast_fusion.2, f32[4,512]{1,0:T(4,128)S(1)} %bitcast.138, pred[512,512]{0,1:T(8,128)(4,1)S(1)} %broadcast_compare_fusion.2), kind=kLoop, calls=%fused_computation.12.clone.1 | loop fusion | flops 6289408 | bytes 4489216 | tf_op jit(solution)/shard_map/while/body/eval_jaxpr/reduce_sum | solution.py:86
  184.3 3.5 %fusion.79 = f32[4,512,64]{1,2,0:T(8,128)S(1)} fusion(bf16[512,4,64]{0,2,1:T(8,128)(2,1)S(1)} %bitcast.132, f32[4,512,512]{2,1,0:T(8,128)} %get-tuple-element.330, f32[4,512]{1,0:T(4,128)S(1)} %select_maximum_fusion.2, f32[4,512]{1,0:T(4,128)S(1)} %dynamic-slice_bitcast_fusion.2, f32[4,512]{1,0:T(4,128)S(1)} %bitcast.139, ...), kind=kOutput, calls=%fused_computation.15.clone.1 | convolution fusion | flops 140902400 | bytes 5799937 | tf_op jit(solution)/shard_map/while/body/eval_jaxpr/hqk,khd->hqd/dot_general | solution.py:87
  189.0 3.1 %fusion.76 = (f32[4,512]{1,0:T(4,128)S(1)}, f32[4,512,512]{2,1,0:T(8,128)}) fusion(f32[4,512]{1,0:T(4,128)S(1)} %dynamic-slice_bitcast_fusion.2, f32[4,512]{1,0:T(4,128)S(1)} %bitcast.137, pred[512,512]{0,1:T(8,128)(4,1)S(1)} %broadcast_compare_fusion.2, bf16[512,4,64]{0,2,1:T(8,128)(2,1)S(1)} %bitcast.131, ...), kind=kOutput, calls=%fused_computation.7.clone.1 | convolution fusion | flops 139458560 | bytes 5005312 | tf_op jit(solution)/shard_map/while/body/eval_jaxpr/qhd,khd->hqk/dot_general | solution.py:77
  192.1 2.9 %fusion.77 = f32[4,512]{1,0:T(4,128)S(1)} fusion(f32[4,512,512]{2,1,0:T(8,128)} %get-tuple-element.330, f32[4,512]{1,0:T(4,128)S(1)} %select_maximum_fusion.2, f32[4,512]{1,0:T(4,128)S(1)} %dynamic-slice_bitcast_fusion.2, f32[4,512]{1,0:T(4,128)S(1)} %bitcast.138, pred[512,512]{0,1:T(8,128)(4,1)S(1)} %broadcast_compare_fusion.2), kind=kLoop, calls=%fused_computation.12.clone.1 | loop fusion | flops 6289408 | bytes 4489216 | tf_op jit(solution)/shard_map/while/body/eval_jaxpr/reduce_sum | solution.py:86
  196.2 3.5 %fusion.79 = f32[4,512,64]{1,2,0:T(8,128)S(1)} fusion(bf16[512,4,64]{0,2,1:T(8,128)(2,1)S(1)} %bitcast.132, f32[4,512,512]{2,1,0:T(8,128)} %get-tuple-element.330, f32[4,512]{1,0:T(4,128)S(1)} %select_maximum_fusion.2, f32[4,512]{1,0:T(4,128)S(1)} %dynamic-slice_bitcast_fusion.2, f32[4,512]{1,0:T(4,128)S(1)} %bitcast.139, ...), kind=kOutput, calls=%fused_computation.15.clone.1 | convolution fusion | flops 140902400 | bytes 5799937 | tf_op jit(solution)/shard_map/while/body/eval_jaxpr/hqk,khd->hqd/dot_general | solution.py:87
  201.0 3.1 %fusion.76 = (f32[4,512]{1,0:T(4,128)S(1)}, f32[4,512,512]{2,1,0:T(8,128)}) fusion(f32[4,512]{1,0:T(4,128)S(1)} %dynamic-slice_bitcast_fusion.2, f32[4,512]{1,0:T(4,128)S(1)} %bitcast.137, pred[512,512]{0,1:T(8,128)(4,1)S(1)} %broadcast_compare_fusion.2, bf16[512,4,64]{0,2,1:T(8,128)(2,1)S(1)} %bitcast.131, ...), kind=kOutput, calls=%fused_computation.7.clone.1 | convolution fusion | flops 139458560 | bytes 5005312 | tf_op jit(solution)/shard_map/while/body/eval_jaxpr/qhd,khd->hqk/dot_general | solution.py:77
  204.1 2.9 %fusion.77 = f32[4,512]{1,0:T(4,128)S(1)} fusion(f32[4,512,512]{2,1,0:T(8,128)} %get-tuple-element.330, f32[4,512]{1,0:T(4,128)S(1)} %select_maximum_fusion.2, f32[4,512]{1,0:T(4,128)S(1)} %dynamic-slice_bitcast_fusion.2, f32[4,512]{1,0:T(4,128)S(1)} %bitcast.138, pred[512,512]{0,1:T(8,128)(4,1)S(1)} %broadcast_compare_fusion.2), kind=kLoop, calls=%fused_computation.12.clone.1 | loop fusion | flops 6289408 | bytes 4489216 | tf_op jit(solution)/shard_map/while/body/eval_jaxpr/reduce_sum | solution.py:86
  208.1 3.5 %fusion.79 = f32[4,512,64]{1,2,0:T(8,128)S(1)} fusion(bf16[512,4,64]{0,2,1:T(8,128)(2,1)S(1)} %bitcast.132, f32[4,512,512]{2,1,0:T(8,128)} %get-tuple-element.330, f32[4,512]{1,0:T(4,128)S(1)} %select_maximum_fusion.2, f32[4,512]{1,0:T(4,128)S(1)} %dynamic-slice_bitcast_fusion.2, f32[4,512]{1,0:T(4,128)S(1)} %bitcast.139, ...), kind=kOutput, calls=%fused_computation.15.clone.1 | convolution fusion | flops 140902400 | bytes 5799937 | tf_op jit(solution)/shard_map/while/body/eval_jaxpr/hqk,khd->hqd/dot_general | solution.py:87
  212.9 3.1 %fusion.76 = (f32[4,512]{1,0:T(4,128)S(1)}, f32[4,512,512]{2,1,0:T(8,128)}) fusion(f32[4,512]{1,0:T(4,128)S(1)} %dynamic-slice_bitcast_fusion.2, f32[4,512]{1,0:T(4,128)S(1)} %bitcast.137, pred[512,512]{0,1:T(8,128)(4,1)S(1)} %broadcast_compare_fusion.2, bf16[512,4,64]{0,2,1:T(8,128)(2,1)S(1)} %bitcast.131, ...), kind=kOutput, calls=%fused_computation.7.clone.1 | convolution fusion | flops 139458560 | bytes 5005312 | tf_op jit(solution)/shard_map/while/body/eval_jaxpr/qhd,khd->hqk/dot_general | solution.py:77
  216.0 2.9 %fusion.77 = f32[4,512]{1,0:T(4,128)S(1)} fusion(f32[4,512,512]{2,1,0:T(8,128)} %get-tuple-element.330, f32[4,512]{1,0:T(4,128)S(1)} %select_maximum_fusion.2, f32[4,512]{1,0:T(4,128)S(1)} %dynamic-slice_bitcast_fusion.2, f32[4,512]{1,0:T(4,128)S(1)} %bitcast.138, pred[512,512]{0,1:T(8,128)(4,1)S(1)} %broadcast_compare_fusion.2), kind=kLoop, calls=%fused_computation.12.clone.1 | loop fusion | flops 6289408 | bytes 4489216 | tf_op jit(solution)/shard_map/while/body/eval_jaxpr/reduce_sum | solution.py:86
  220.1 3.5 %fusion.79 = f32[4,512,64]{1,2,0:T(8,128)S(1)} fusion(bf16[512,4,64]{0,2,1:T(8,128)(2,1)S(1)} %bitcast.132, f32[4,512,512]{2,1,0:T(8,128)} %get-tuple-element.330, f32[4,512]{1,0:T(4,128)S(1)} %select_maximum_fusion.2, f32[4,512]{1,0:T(4,128)S(1)} %dynamic-slice_bitcast_fusion.2, f32[4,512]{1,0:T(4,128)S(1)} %bitcast.139, ...), kind=kOutput, calls=%fused_computation.15.clone.1 | convolution fusion | flops 140902400 | bytes 5799937 | tf_op jit(solution)/shard_map/while/body/eval_jaxpr/hqk,khd->hqd/dot_general | solution.py:87
  224.6 3.5 %all-to-all-start.1 = ((bf16[8,48,512]{2,1,0:T(8,128)(2,1)}), bf16[8,48,512]{2,1,0:T(8,128)(2,1)S(1)}, u32[]{:S(2)}, u32[]{:S(2)}) async-start(bf16[8,48,512]{2,1,0:T(8,128)(2,1)} %bitcast.135), calls=%async_computation.2 | async-start | bytes 786432 | tf_op jit(solution)/shard_map/all_to_all | solution.py:149
  228.2 22.6 %all-gather.9.cloned.1.call-done = bf16[512,1024]{0,1:T(8,128)(2,1)} async-done(((bf16[512,256]{0,1:T(8,128)(2,1)}), bf16[512,1024]{0,1:T(8,128)(2,1)}) %all-gather.9.cloned.1.call-update) | async-done | bytes 1048592 | tf_op jit(solution)/shard_map/all_gather | solution.py:103
  250.8 3.1 %convolution_convert_fusion.1 = bf16[512,512]{1,0:T(8,128)(2,1)} fusion(bf16[512,1024]{0,1:T(8,128)(2,1)} %all-gather.9.cloned.1.call-done, bf16[1024,512]{1,0:T(8,128)(2,1)} %param.28), kind=kOutput, calls=%fused_computation.38 | convolution fusion | flops 537133056 | bytes 2621440 | tf_op jit(solution)/shard_map/dot_general | solution.py:102
  253.8 1.2 gather_fusion.1
  255.3 1.4 multiply_reduce_fusion
  (138 shorter events, 23.2 us)
Async XLA Ops:
  7.2 62.1 %copy-start = (bf16[1,256,2048]{2,1,0:T(8,128)(2,1)S(1)}, bf16[1,256,2048]{2,1,0:T(8,128)(2,1)}, u32[]{:S(2)}) copy-start(bf16[1,256,2048]{2,1,0:T(8,128)(2,1)} %param.35) | copy-start | bytes 3145732
  7.2 59.9 %all-gather.11.cloned.1.call-start = ((), (), s32[]{:S(2)}) async-start(), calls=%async_computation.6 | async-start | bytes 1966080 | tf_op jit(solution)/shard_map/all_gather | solution.py:132
  15.8 21.5 %copy-start.6 = (f32[64]{0:T(128)S(1)}, f32[64]{0:T(128)}, u32[]{:S(2)}) copy-start(f32[64]{0:T(128)} %param.25) | copy-start | bytes 772
  15.8 23.8 %copy-start.8 = (f32[2048]{0:T(1024)S(1)}, f32[2048]{0:T(1024)}, u32[]{:S(2)}) copy-start(f32[2048]{0:T(1024)} %param.20) | copy-start | bytes 24580
  37.2 60.6 %all-gather.5.cloned.1.call-start = ((), (), s32[]{:S(2)}) async-start(), calls=%async_computation.3 | async-start | bytes 2359296 | tf_op jit(solution)/shard_map/all_gather | solution.py:61
  37.4 6.0 %copy-start.1 = (bf16[512,2048]{1,0:T(8,128)(2,1)S(1)}, bf16[512,2048]{1,0:T(8,128)(2,1)}, u32[]{:S(2)}) copy-start(bf16[512,2048]{1,0:T(8,128)(2,1)} %param.19) | copy-start | bytes 6291460
  42.4 3.8 %copy-start.5 = (f32[256]{0:T(256)S(1)}, f32[256]{0:T(256)}, u32[]{:S(2)}) copy-start(f32[256]{0:T(256)} %param.27) | copy-start | bytes 3076
  42.4 3.8 %copy-start.3 = (f32[512,4]{0,1:T(4,128)S(1)}, f32[512,4]{0,1:T(4,128)}, u32[]{:S(2)}) copy-start(f32[512,4]{0,1:T(4,128)} %param.26) | copy-start | bytes 24580
  43.3 84.7 %all-gather.7.cloned.1.call-start = ((), (), s32[]{:S(2)}) async-start(), calls=%async_computation.4 | async-start | bytes 2359296 | tf_op jit(solution)/shard_map/all_gather | solution.py:62
  46.1 16.4 %copy-start.7 = (f32[64]{0:T(128)S(1)}, f32[64]{0:T(128)}, u32[]{:S(2)}) copy-start(f32[64]{0:T(128)} %param.24) | copy-start | bytes 772
  46.1 178.5 %reduce-scatter.2.cloned.1.call-start = ((), (), s32[]{:S(2)}) async-start(), calls=%async_computation.7 | async-start | bytes 1966080 | tf_op jit(solution)/shard_map/reduce_scatter | solution.py:145
  69.3 58.7 %copy-start.2 = (f32[4,512,64]{1,2,0:T(8,128)S(1)}, f32[4,512,64]{1,2,0:T(8,128)}, u32[]{:S(2)}) copy-start(f32[4,512,64]{1,2,0:T(8,128)} %custom-call.2) | copy-start | bytes 1572868
  74.1 176.6 %all-gather.9.cloned.1.call-start = ((), (), s32[]{:S(2)}) async-start(), calls=%async_computation.5 | async-start | bytes 1310720 | tf_op jit(solution)/shard_map/all_gather | solution.py:103
  128.0 100.0 %copy-start.4 = (f32[128,2]{0,1:T(2,128)S(1)}, f32[128,2]{0,1:T(2,128)}, u32[]{:S(2)}) copy-start(f32[128,2]{0,1:T(2,128)} %param.32) | copy-start | bytes 3076
  224.6 29.3 %all-to-all-start.1 = ((bf16[8,48,512]{2,1,0:T(8,128)(2,1)}), bf16[8,48,512]{2,1,0:T(8,128)(2,1)S(1)}, u32[]{:S(2)}, u32[]{:S(2)}) async-start(bf16[8,48,512]{2,1,0:T(8,128)(2,1)} %bitcast.135), calls=%async_computation.2 | async-start | bytes 786432 | tf_op jit(solution)/shard_map/all_to_all | solution.py:149
Sparse Core Ops, SparseCore 0:
  37.3 29.6 all-gather.10
  68.6 29.1 all-gather.4
  99.4 28.5 all-gather.6
  130.8 30.5 reduce-scatter.1
  224.6 26.0 all-gather.8
where the time goes:
time: 265 us; the launch traced here: 263 us
  waiting for transfers between devices  80.8 us (30%)
  matrix products  70.6 us (27%)
  other arithmetic  34.9 us (13%)
  blocking collectives  32.8 us (12%)
  local copies, waits for them, and re-layouts  25.7 us (10%)
  between operations  14.1 us (5%)
  starting transfers between devices  3.85 us (1%)
    all_gather x1, waiting for transfers between devices, body(): value_piece = lax.all_gather(value_rows, 'ep', axis=0, tiled=True)  30.2 us
    dot_general x8, matrix products, block_step(): jnp.einsum('hqk,khd->hqd', expo_scores.astype(jnp.bfloat16), value_block,...  28.1 us
    dot_general x8, matrix products, block_step(): jnp.einsum('qhd,khd->hqk', queries, key_block, preferred_element_type=jnp...  24.7 us
    all_gather x1, waiting for transfers between devices, body(): key_piece = lax.all_gather(key_rows, 'ep', axis=0, tiled=True)  23.4 us
    reduce_sum x8, other arithmetic, block_step(): running_sum = running_sum * rescale + jnp.sum(expo_scores, axis=2)  23.4 us
    all_gather x1, waiting for transfers between devices, body(): lax.all_gather(head_out, 'tp', axis=1, tiled=True)  22.6 us
    all_to_all x1, blocking collectives, body(): lax.all_to_all(share_part, 'ep', split_axis=0, concat_axis=0, tiled=True)  18.8 us
    all_gather x1, blocking collectives, body(): all_gates = lax.all_gather(log_cache, 'ep', axis=0, tiled=True)  14 us
  transfers between devices with their start and end apart: 6, of which 4 were waited for; matrix products, arithmetic and copies ran while one was open for 45% of the time, Pallas kernels for 0%

commit v1 on v0

--- a/solution.py
+++ b/solution.py
@@ -49,7 +49,6 @@
         .reshape(tok_rows, local_heads * HD)
     )
     value_rows = project(value_weight).astype(jnp.bfloat16).reshape(tok_rows, local_heads * HD)
-    all_gates = lax.all_gather(log_cache, "ep", axis=0, tiled=True)
     query_pos = lax.axis_index("ep") * tok_rows + jnp.arange(tok_rows, dtype=jnp.int32)
     query_gates = jnp.transpose(log_cache)[:, :, None]
     score_scale = HD ** (-0.5)
@@ -58,7 +57,11 @@
         jnp.zeros((local_heads, tok_rows), jnp.float32),
         jnp.zeros((local_heads, tok_rows, HD), jnp.float32),
     )
-    key_piece = lax.all_gather(key_rows, "ep", axis=0, tiled=True)
+    all_gates, key_piece = jnp.split(
+        lax.all_gather(jnp.concatenate([log_cache, key_rows], axis=1), "ep", axis=0, tiled=True),
+        [log_cache.shape[1]],
+        axis=1,
+    )
     value_piece = lax.all_gather(value_rows, "ep", axis=0, tiled=True)
     span_len = key_piece.shape[0]
     block_len = math.gcd(span_len, 512)

time: 265 us -> 280 us (1.057)
  waiting for transfers between devices: 80.8 us -> 106 us
  blocking collectives: 32.8 us -> 18.8 us
  local copies, waits for them, and re-layouts: 25.7 us -> 29.8 us
    all_gather x1, waiting for transfers between devices: 23.4 us -> 42.3 us  [body(): lax.all_gather(jnp.concatenate([log_cache, key_rows], axis=1), 'ep', axis...]
    all_gather x1, waiting for transfers between devices: 22.6 us -> 7.39 us  [body(): lax.all_gather(head_out, 'tp', axis=1, tiled=True)]
    all_gather x1 -> x0, blocking collectives: 14 us -> none  [body(): all_gates = lax.all_gather(log_cache, 'ep', axis=0, tiled=True)]
    all_gather x1, waiting for transfers between devices: 4.48 us -> 18.3 us  [body(): piece_now = lax.all_gather(arrived, 'tp', axis=2, tiled=True)]
    all_to_all x1, waiting for transfers between devices: 0.01 us -> 12.3 us  [body(): lax.all_to_all(summed.reshape(expert_count, capacity, out_cols), 'ep', sp...]
    all_gather x1, waiting for transfers between devices: 30.2 us -> 25.5 us  [body(): value_piece = lax.all_gather(value_rows, 'ep', axis=0, tiled=True)]
    split x0 -> x3, local copies, waits for them, and re-layouts: none -> 4.1 us  [body(): jnp.split(lax.all_gather(jnp.concatenate([log_cache, key_rows], axis=1),...]
  transfers between devices with their start and end apart: 6 -> 6, of which waited for: 4 -> 5; matrix products, arithmetic and copies ran while one was open for 45% -> 43% of each run, Pallas kernels for 0% -> 0%
where the time goes in v1:
time: 280 us; the launch traced here: 279 us
  waiting for transfers between devices  106 us (38%)
  matrix products  70.6 us (25%)
  other arithmetic  34.9 us (12%)
  local copies, waits for them, and re-layouts  29.8 us (11%)
  blocking collectives  18.8 us (7%)
  between operations  14.1 us (5%)
  starting transfers between devices  3.85 us (1%)
    all_gather x1, waiting for transfers between devices, body(): lax.all_gather(jnp.concatenate([log_cache, key_rows], axis=1), 'ep', axis...  42.3 us
    dot_general x8, matrix products, block_step(): jnp.einsum('hqk,khd->hqd', expo_scores.astype(jnp.bfloat16), value_block,...  28.1 us
    all_gather x1, waiting for transfers between devices, body(): value_piece = lax.all_gather(value_rows, 'ep', axis=0, tiled=True)  25.5 us
    dot_general x8, matrix products, block_step(): jnp.einsum('qhd,khd->hqk', queries, key_block, preferred_element_type=jnp...  24.7 us
    reduce_sum x8, other arithmetic, block_step(): running_sum = running_sum * rescale + jnp.sum(expo_scores, axis=2)  23.4 us
    all_to_all x1, blocking collectives, body(): lax.all_to_all(share_part, 'ep', split_axis=0, concat_axis=0, tiled=True)  18.8 us
    all_gather x1, waiting for transfers between devices, body(): piece_now = lax.all_gather(arrived, 'tp', axis=2, tiled=True)  18.3 us
    all_to_all x1, waiting for transfers between devices, body(): lax.all_to_all(summed.reshape(expert_count, capacity, out_cols), 'ep', sp...  12.3 us
  transfers between devices with their start and end apart: 6, of which 5 were waited for; matrix products, arithmetic and copies ran while one was open for 43% of the time, Pallas kernels for 0%

profile of v1, /device:TPU:0, one launch (start us, length us, event | category | flops | bytes accessed | tf_op | source)
XLA Modules:
  0.0 278.5 jit_solution(13499023942574114437)
XLA Ops:
  10.3 1.4 scatter_custom_fusion.1
  11.7 1.2 fusion.23
  13.0 1.5 scatter_custom_fusion
  14.5 1.2 fusion.25
  15.8 2.5 gather_fusion
  18.4 18.8 %all_to_all.10 = bf16[8,48,512]{2,1,0:T(8,128)(2,1)} all-to-all(bf16[8,48,512]{2,1,0:T(8,128)(2,1)S(1)} %dynamic-slice_select_fusion), channel_id=1, replica_groups=mesh['ep'=8,'tp'=4] {'ep'}, dimensions={0} | all-to-all | bytes 786432 | tf_op jit(solution)/shard_map/all_to_all | solution.py:134
  37.4 2.1 fusion.16
  39.5 2.9 %bitcast_reduce_fusion = (f32[512,4]{0,1:T(4,128)S(1)}, f32[512,256]{0,1:T(8,128)S(1)}) fusion(bf16[2048,256]{1,0:T(8,128)(2,1)} %param.22, bf16[512,2048]{1,0:T(8,128)(2,1)} %param.19, f32[2048]{0:T(1024)S(1)} %copy-done.8, f32[512]{0:T(512)S(1)} %add_rsqrt_fusion.3), kind=kOutput, calls=%fused_computation.60 | convolution fusion | flops 541325312 | bytes 3688448 | tf_op jit(solution)/shard_map/dot_general | solution.py:41
  43.5 2.7 convolution_convert_fusion.2
  46.4 2.2 multiply_reduce_fusion.1
  48.7 18.3 %all-gather.11.cloned.1.call-done = bf16[8,48,2048]{2,1,0:T(8,128)(2,1)} async-done(((bf16[8,48,512]{2,1,0:T(8,128)(2,1)}), bf16[8,48,2048]{2,1,0:T(8,128)(2,1)}) %all-gather.11.cloned.1.call-update) | async-done | bytes 1572880 | tf_op jit(solution)/shard_map/all_gather | solution.py:135
  67.0 2.3 convolution_bitcast_fusion.1
  69.3 4.7 %fusion.19 = bf16[8,1,48,2048]{3,2,0,1:T(8,128)(2,1)} fusion(bf16[1,256,2048]{2,1,0:T(8,128)(2,1)S(1)} %copy-done, bf16[8,48,2048]{2,1,0:T(8,128)(2,1)} %all-gather.11.cloned.1.call-done, bf16[1,2048,256]{2,1,0:T(8,128)(2,1)} %param.34, f32[8,1,48,256]{3,2,0,1:T(8,128)S(1)} %convolution_bitcast_fusion.1), kind=kOutput, calls=%fused_computation.35 | convolution fusion | flops 806682624 | bytes 5636096 | tf_op jit(solution)/shard_map/sjcf,jfd->sjcd/dot_general | solution.py:145
  74.3 42.3 %all-gather.5.cloned.1.call-done = f32[4096,260]{0,1:T(8,128)} async-done(((f32[512,260]{0,1:T(8,128)}), f32[4096,260]{0,1:T(8,128)}) %all-gather.5.cloned.1.call-update) | async-done | bytes 4259856 | tf_op jit(solution)/shard_map/all_gather | solution.py:61
  116.6 4.1 %split.8 = bf16[4096,256]{0,1:T(8,128)(2,1)} slice(f32[4096,260]{0,1:T(8,128)} %all-gather.5.cloned.1.call-done), slice={[0:4096], [4:260]} | slice | bytes 4194304 | tf_op jit(solution)/shard_map/split | solution.py:60
  120.7 25.5 %all-gather.7.cloned.1.call-done = bf16[4096,256]{1,0:T(8,128)(2,1)} async-done(((bf16[512,256]{1,0:T(8,128)(2,1)}), bf16[4096,256]{1,0:T(8,128)(2,1)}) %all-gather.7.cloned.1.call-update) | async-done | bytes 2097168 | tf_op jit(solution)/shard_map/all_gather | solution.py:65
  146.2 95.6 %while.18 = (s32[]{:T(128)}, f32[4,512]{1,0:T(4,128)S(1)}, f32[4,512]{1,0:T(4,128)S(1)}, f32[4,512,64]{1,2,0:T(8,128)S(1)}, bf16[4096,256]{0,1:T(8,128)(2,1)}, /...) while((s32[]{:T(128)}, f32[4,512]{1,0:T(4,128)S(1)}, ...), condition=%wide.region_6.7_spmd.clone, body=%wide.region_3.6_spmd.clone.sunk | while | flops 286927872 | bytes 17244372 | solution.py:98
  147.4 3.1 %fusion.77 = (f32[4,512]{1,0:T(4,128)S(1)}, f32[4,512,512]{2,1,0:T(8,128)}) fusion(f32[4,512]{1,0:T(4,128)S(1)} %dynamic-slice_bitcast_fusion.2, f32[4,512]{1,0:T(4,128)S(1)} %bitcast.139, pred[512,512]{0,1:T(8,128)(4,1)S(1)} %broadcast_compare_fusion.2, bf16[512,4,64]{0,2,1:T(8,128)(2,1)S(1)} %bitcast.133, ...), kind=kOutput, calls=%fused_computation.7.clone.1 | convolution fusion | flops 139458560 | bytes 5005312 | tf_op jit(solution)/shard_map/while/body/eval_jaxpr/qhd,khd->hqk/dot_general | solution.py:80
  150.5 2.9 %fusion.78 = f32[4,512]{1,0:T(4,128)S(1)} fusion(f32[4,512,512]{2,1,0:T(8,128)} %get-tuple-element.330, f32[4,512]{1,0:T(4,128)S(1)} %select_maximum_fusion.2, f32[4,512]{1,0:T(4,128)S(1)} %dynamic-slice_bitcast_fusion.2, f32[4,512]{1,0:T(4,128)S(1)} %bitcast.140, pred[512,512]{0,1:T(8,128)(4,1)S(1)} %broadcast_compare_fusion.2), kind=kLoop, calls=%fused_computation.12.clone.1 | loop fusion | flops 6289408 | bytes 4489216 | tf_op jit(solution)/shard_map/while/body/eval_jaxpr/reduce_sum | solution.py:89
  154.6 3.5 %fusion.80 = f32[4,512,64]{1,2,0:T(8,128)S(1)} fusion(bf16[512,4,64]{0,2,1:T(8,128)(2,1)S(1)} %bitcast.134, f32[4,512,512]{2,1,0:T(8,128)} %get-tuple-element.330, f32[4,512]{1,0:T(4,128)S(1)} %select_maximum_fusion.2, f32[4,512]{1,0:T(4,128)S(1)} %dynamic-slice_bitcast_fusion.2, f32[4,512]{1,0:T(4,128)S(1)} %bitcast.141, ...), kind=kOutput, calls=%fused_computation.15.clone.1 | convolution fusion | flops 140902400 | bytes 5799937 | tf_op jit(solution)/shard_map/while/body/eval_jaxpr/hqk,khd->hqd/dot_general | solution.py:90
  159.4 3.1 %fusion.77 = (f32[4,512]{1,0:T(4,128)S(1)}, f32[4,512,512]{2,1,0:T(8,128)}) fusion(f32[4,512]{1,0:T(4,128)S(1)} %dynamic-slice_bitcast_fusion.2, f32[4,512]{1,0:T(4,128)S(1)} %bitcast.139, pred[512,512]{0,1:T(8,128)(4,1)S(1)} %broadcast_compare_fusion.2, bf16[512,4,64]{0,2,1:T(8,128)(2,1)S(1)} %bitcast.133, ...), kind=kOutput, calls=%fused_computation.7.clone.1 | convolution fusion | flops 139458560 | bytes 5005312 | tf_op jit(solution)/shard_map/while/body/eval_jaxpr/qhd,khd->hqk/dot_general | solution.py:80
  162.5 3.0 %fusion.78 = f32[4,512]{1,0:T(4,128)S(1)} fusion(f32[4,512,512]{2,1,0:T(8,128)} %get-tuple-element.330, f32[4,512]{1,0:T(4,128)S(1)} %select_maximum_fusion.2, f32[4,512]{1,0:T(4,128)S(1)} %dynamic-slice_bitcast_fusion.2, f32[4,512]{1,0:T(4,128)S(1)} %bitcast.140, pred[512,512]{0,1:T(8,128)(4,1)S(1)} %broadcast_compare_fusion.2), kind=kLoop, calls=%fused_computation.12.clone.1 | loop fusion | flops 6289408 | bytes 4489216 | tf_op jit(solution)/shard_map/while/body/eval_jaxpr/reduce_sum | solution.py:89
  165.5 1.0 constant_dynamic-slice_fusion.5
  166.6 3.5 %fusion.80 = f32[4,512,64]{1,2,0:T(8,128)S(1)} fusion(bf16[512,4,64]{0,2,1:T(8,128)(2,1)S(1)} %bitcast.134, f32[4,512,512]{2,1,0:T(8,128)} %get-tuple-element.330, f32[4,512]{1,0:T(4,128)S(1)} %select_maximum_fusion.2, f32[4,512]{1,0:T(4,128)S(1)} %dynamic-slice_bitcast_fusion.2, f32[4,512]{1,0:T(4,128)S(1)} %bitcast.141, ...), kind=kOutput, calls=%fused_computation.15.clone.1 | convolution fusion | flops 140902400 | bytes 5799937 | tf_op jit(solution)/shard_map/while/body/eval_jaxpr/hqk,khd->hqd/dot_general | solution.py:90
  171.4 3.1 %fusion.77 = (f32[4,512]{1,0:T(4,128)S(1)}, f32[4,512,512]{2,1,0:T(8,128)}) fusion(f32[4,512]{1,0:T(4,128)S(1)} %dynamic-slice_bitcast_fusion.2, f32[4,512]{1,0:T(4,128)S(1)} %bitcast.139, pred[512,512]{0,1:T(8,128)(4,1)S(1)} %broadcast_compare_fusion.2, bf16[512,4,64]{0,2,1:T(8,128)(2,1)S(1)} %bitcast.133, ...), kind=kOutput, calls=%fused_computation.7.clone.1 | convolution fusion | flops 139458560 | bytes 5005312 | tf_op jit(solution)/shard_map/while/body/eval_jaxpr/qhd,khd->hqk/dot_general | solution.py:80
  174.5 2.9 %fusion.78 = f32[4,512]{1,0:T(4,128)S(1)} fusion(f32[4,512,512]{2,1,0:T(8,128)} %get-tuple-element.330, f32[4,512]{1,0:T(4,128)S(1)} %select_maximum_fusion.2, f32[4,512]{1,0:T(4,128)S(1)} %dynamic-slice_bitcast_fusion.2, f32[4,512]{1,0:T(4,128)S(1)} %bitcast.140, pred[512,512]{0,1:T(8,128)(4,1)S(1)} %broadcast_compare_fusion.2), kind=kLoop, calls=%fused_computation.12.clone.1 | loop fusion | flops 6289408 | bytes 4489216 | tf_op jit(solution)/shard_map/while/body/eval_jaxpr/reduce_sum | solution.py:89
  178.6 3.6 %fusion.80 = f32[4,512,64]{1,2,0:T(8,128)S(1)} fusion(bf16[512,4,64]{0,2,1:T(8,128)(2,1)S(1)} %bitcast.134, f32[4,512,512]{2,1,0:T(8,128)} %get-tuple-element.330, f32[4,512]{1,0:T(4,128)S(1)} %select_maximum_fusion.2, f32[4,512]{1,0:T(4,128)S(1)} %dynamic-slice_bitcast_fusion.2, f32[4,512]{1,0:T(4,128)S(1)} %bitcast.141, ...), kind=kOutput, calls=%fused_computation.15.clone.1 | convolution fusion | flops 140902400 | bytes 5799937 | tf_op jit(solution)/shard_map/while/body/eval_jaxpr/hqk,khd->hqd/dot_general | solution.py:90
  183.4 3.1 %fusion.77 = (f32[4,512]{1,0:T(4,128)S(1)}, f32[4,512,512]{2,1,0:T(8,128)}) fusion(f32[4,512]{1,0:T(4,128)S(1)} %dynamic-slice_bitcast_fusion.2, f32[4,512]{1,0:T(4,128)S(1)} %bitcast.139, pred[512,512]{0,1:T(8,128)(4,1)S(1)} %broadcast_compare_fusion.2, bf16[512,4,64]{0,2,1:T(8,128)(2,1)S(1)} %bitcast.133, ...), kind=kOutput, calls=%fused_computation.7.clone.1 | convolution fusion | flops 139458560 | bytes 5005312 | tf_op jit(solution)/shard_map/while/body/eval_jaxpr/qhd,khd->hqk/dot_general | solution.py:80
  186.5 2.9 %fusion.78 = f32[4,512]{1,0:T(4,128)S(1)} fusion(f32[4,512,512]{2,1,0:T(8,128)} %get-tuple-element.330, f32[4,512]{1,0:T(4,128)S(1)} %select_maximum_fusion.2, f32[4,512]{1,0:T(4,128)S(1)} %dynamic-slice_bitcast_fusion.2, f32[4,512]{1,0:T(4,128)S(1)} %bitcast.140, pred[512,512]{0,1:T(8,128)(4,1)S(1)} %broadcast_compare_fusion.2), kind=kLoop, calls=%fused_computation.12.clone.1 | loop fusion | flops 6289408 | bytes 4489216 | tf_op jit(solution)/shard_map/while/body/eval_jaxpr/reduce_sum | solution.py:89
  190.5 3.5 %fusion.80 = f32[4,512,64]{1,2,0:T(8,128)S(1)} fusion(bf16[512,4,64]{0,2,1:T(8,128)(2,1)S(1)} %bitcast.134, f32[4,512,512]{2,1,0:T(8,128)} %get-tuple-element.330, f32[4,512]{1,0:T(4,128)S(1)} %select_maximum_fusion.2, f32[4,512]{1,0:T(4,128)S(1)} %dynamic-slice_bitcast_fusion.2, f32[4,512]{1,0:T(4,128)S(1)} %bitcast.141, ...), kind=kOutput, calls=%fused_computation.15.clone.1 | convolution fusion | flops 140902400 | bytes 5799937 | tf_op jit(solution)/shard_map/while/body/eval_jaxpr/hqk,khd->hqd/dot_general | solution.py:90
  195.3 3.1 %fusion.77 = (f32[4,512]{1,0:T(4,128)S(1)}, f32[4,512,512]{2,1,0:T(8,128)}) fusion(f32[4,512]{1,0:T(4,128)S(1)} %dynamic-slice_bitcast_fusion.2, f32[4,512]{1,0:T(4,128)S(1)} %bitcast.139, pred[512,512]{0,1:T(8,128)(4,1)S(1)} %broadcast_compare_fusion.2, bf16[512,4,64]{0,2,1:T(8,128)(2,1)S(1)} %bitcast.133, ...), kind=kOutput, calls=%fused_computation.7.clone.1 | convolution fusion | flops 139458560 | bytes 5005312 | tf_op jit(solution)/shard_map/while/body/eval_jaxpr/qhd,khd->hqk/dot_general | solution.py:80
  198.4 2.9 %fusion.78 = f32[4,512]{1,0:T(4,128)S(1)} fusion(f32[4,512,512]{2,1,0:T(8,128)} %get-tuple-element.330, f32[4,512]{1,0:T(4,128)S(1)} %select_maximum_fusion.2, f32[4,512]{1,0:T(4,128)S(1)} %dynamic-slice_bitcast_fusion.2, f32[4,512]{1,0:T(4,128)S(1)} %bitcast.140, pred[512,512]{0,1:T(8,128)(4,1)S(1)} %broadcast_compare_fusion.2), kind=kLoop, calls=%fused_computation.12.clone.1 | loop fusion | flops 6289408 | bytes 4489216 | tf_op jit(solution)/shard_map/while/body/eval_jaxpr/reduce_sum | solution.py:89
  202.5 3.5 %fusion.80 = f32[4,512,64]{1,2,0:T(8,128)S(1)} fusion(bf16[512,4,64]{0,2,1:T(8,128)(2,1)S(1)} %bitcast.134, f32[4,512,512]{2,1,0:T(8,128)} %get-tuple-element.330, f32[4,512]{1,0:T(4,128)S(1)} %select_maximum_fusion.2, f32[4,512]{1,0:T(4,128)S(1)} %dynamic-slice_bitcast_fusion.2, f32[4,512]{1,0:T(4,128)S(1)} %bitcast.141, ...), kind=kOutput, calls=%fused_computation.15.clone.1 | convolution fusion | flops 140902400 | bytes 5799937 | tf_op jit(solution)/shard_map/while/body/eval_jaxpr/hqk,khd->hqd/dot_general | solution.py:90
  207.2 3.1 %fusion.77 = (f32[4,512]{1,0:T(4,128)S(1)}, f32[4,512,512]{2,1,0:T(8,128)}) fusion(f32[4,512]{1,0:T(4,128)S(1)} %dynamic-slice_bitcast_fusion.2, f32[4,512]{1,0:T(4,128)S(1)} %bitcast.139, pred[512,512]{0,1:T(8,128)(4,1)S(1)} %broadcast_compare_fusion.2, bf16[512,4,64]{0,2,1:T(8,128)(2,1)S(1)} %bitcast.133, ...), kind=kOutput, calls=%fused_computation.7.clone.1 | convolution fusion | flops 139458560 | bytes 5005312 | tf_op jit(solution)/shard_map/while/body/eval_jaxpr/qhd,khd->hqk/dot_general | solution.py:80
  210.3 2.9 %fusion.78 = f32[4,512]{1,0:T(4,128)S(1)} fusion(f32[4,512,512]{2,1,0:T(8,128)} %get-tuple-element.330, f32[4,512]{1,0:T(4,128)S(1)} %select_maximum_fusion.2, f32[4,512]{1,0:T(4,128)S(1)} %dynamic-slice_bitcast_fusion.2, f32[4,512]{1,0:T(4,128)S(1)} %bitcast.140, pred[512,512]{0,1:T(8,128)(4,1)S(1)} %broadcast_compare_fusion.2), kind=kLoop, calls=%fused_computation.12.clone.1 | loop fusion | flops 6289408 | bytes 4489216 | tf_op jit(solution)/shard_map/while/body/eval_jaxpr/reduce_sum | solution.py:89
  214.4 3.5 %fusion.80 = f32[4,512,64]{1,2,0:T(8,128)S(1)} fusion(bf16[512,4,64]{0,2,1:T(8,128)(2,1)S(1)} %bitcast.134, f32[4,512,512]{2,1,0:T(8,128)} %get-tuple-element.330, f32[4,512]{1,0:T(4,128)S(1)} %select_maximum_fusion.2, f32[4,512]{1,0:T(4,128)S(1)} %dynamic-slice_bitcast_fusion.2, f32[4,512]{1,0:T(4,128)S(1)} %bitcast.141, ...), kind=kOutput, calls=%fused_computation.15.clone.1 | convolution fusion | flops 140902400 | bytes 5799937 | tf_op jit(solution)/shard_map/while/body/eval_jaxpr/hqk,khd->hqd/dot_general | solution.py:90
  219.2 3.1 %fusion.77 = (f32[4,512]{1,0:T(4,128)S(1)}, f32[4,512,512]{2,1,0:T(8,128)}) fusion(f32[4,512]{1,0:T(4,128)S(1)} %dynamic-slice_bitcast_fusion.2, f32[4,512]{1,0:T(4,128)S(1)} %bitcast.139, pred[512,512]{0,1:T(8,128)(4,1)S(1)} %broadcast_compare_fusion.2, bf16[512,4,64]{0,2,1:T(8,128)(2,1)S(1)} %bitcast.133, ...), kind=kOutput, calls=%fused_computation.7.clone.1 | convolution fusion | flops 139458560 | bytes 5005312 | tf_op jit(solution)/shard_map/while/body/eval_jaxpr/qhd,khd->hqk/dot_general | solution.py:80
  222.3 2.9 %fusion.78 = f32[4,512]{1,0:T(4,128)S(1)} fusion(f32[4,512,512]{2,1,0:T(8,128)} %get-tuple-element.330, f32[4,512]{1,0:T(4,128)S(1)} %select_maximum_fusion.2, f32[4,512]{1,0:T(4,128)S(1)} %dynamic-slice_bitcast_fusion.2, f32[4,512]{1,0:T(4,128)S(1)} %bitcast.140, pred[512,512]{0,1:T(8,128)(4,1)S(1)} %broadcast_compare_fusion.2), kind=kLoop, calls=%fused_computation.12.clone.1 | loop fusion | flops 6289408 | bytes 4489216 | tf_op jit(solution)/shard_map/while/body/eval_jaxpr/reduce_sum | solution.py:89
  226.3 3.5 %fusion.80 = f32[4,512,64]{1,2,0:T(8,128)S(1)} fusion(bf16[512,4,64]{0,2,1:T(8,128)(2,1)S(1)} %bitcast.134, f32[4,512,512]{2,1,0:T(8,128)} %get-tuple-element.330, f32[4,512]{1,0:T(4,128)S(1)} %select_maximum_fusion.2, f32[4,512]{1,0:T(4,128)S(1)} %dynamic-slice_bitcast_fusion.2, f32[4,512]{1,0:T(4,128)S(1)} %bitcast.141, ...), kind=kOutput, calls=%fused_computation.15.clone.1 | convolution fusion | flops 140902400 | bytes 5799937 | tf_op jit(solution)/shard_map/while/body/eval_jaxpr/hqk,khd->hqd/dot_general | solution.py:90
  231.1 3.1 %fusion.77 = (f32[4,512]{1,0:T(4,128)S(1)}, f32[4,512,512]{2,1,0:T(8,128)}) fusion(f32[4,512]{1,0:T(4,128)S(1)} %dynamic-slice_bitcast_fusion.2, f32[4,512]{1,0:T(4,128)S(1)} %bitcast.139, pred[512,512]{0,1:T(8,128)(4,1)S(1)} %broadcast_compare_fusion.2, bf16[512,4,64]{0,2,1:T(8,128)(2,1)S(1)} %bitcast.133, ...), kind=kOutput, calls=%fused_computation.7.clone.1 | convolution fusion | flops 139458560 | bytes 5005312 | tf_op jit(solution)/shard_map/while/body/eval_jaxpr/qhd,khd->hqk/dot_general | solution.py:80
  234.2 2.9 %fusion.78 = f32[4,512]{1,0:T(4,128)S(1)} fusion(f32[4,512,512]{2,1,0:T(8,128)} %get-tuple-element.330, f32[4,512]{1,0:T(4,128)S(1)} %select_maximum_fusion.2, f32[4,512]{1,0:T(4,128)S(1)} %dynamic-slice_bitcast_fusion.2, f32[4,512]{1,0:T(4,128)S(1)} %bitcast.140, pred[512,512]{0,1:T(8,128)(4,1)S(1)} %broadcast_compare_fusion.2), kind=kLoop, calls=%fused_computation.12.clone.1 | loop fusion | flops 6289408 | bytes 4489216 | tf_op jit(solution)/shard_map/while/body/eval_jaxpr/reduce_sum | solution.py:89
  238.3 3.5 %fusion.80 = f32[4,512,64]{1,2,0:T(8,128)S(1)} fusion(bf16[512,4,64]{0,2,1:T(8,128)(2,1)S(1)} %bitcast.134, f32[4,512,512]{2,1,0:T(8,128)} %get-tuple-element.330, f32[4,512]{1,0:T(4,128)S(1)} %select_maximum_fusion.2, f32[4,512]{1,0:T(4,128)S(1)} %dynamic-slice_bitcast_fusion.2, f32[4,512]{1,0:T(4,128)S(1)} %bitcast.141, ...), kind=kOutput, calls=%fused_computation.15.clone.1 | convolution fusion | flops 140902400 | bytes 5799937 | tf_op jit(solution)/shard_map/while/body/eval_jaxpr/hqk,khd->hqd/dot_general | solution.py:90
  242.8 3.5 %all-to-all-start.1 = ((bf16[8,48,512]{2,1,0:T(8,128)(2,1)}), bf16[8,48,512]{2,1,0:T(8,128)(2,1)S(1)}, u32[]{:S(2)}, u32[]{:S(2)}) async-start(bf16[8,48,512]{2,1,0:T(8,128)(2,1)} %bitcast.137), calls=%async_computation.2 | async-start | bytes 786432 | tf_op jit(solution)/shard_map/all_to_all | solution.py:152
  246.4 12.3 %all-to-all-done.1 = bf16[8,48,512]{2,1,0:T(8,128)(2,1)S(1)} async-done(((bf16[8,48,512]{2,1,0:T(8,128)(2,1)}), bf16[8,48,512]{2,1,0:T(8,128)(2,1)S(1)}, u32[]{:S(2)}, u32[]{:S(2)}) %all-to-all-start.1) | async-done | bytes 393248 | tf_op jit(solution)/shard_map/all_to_all | solution.py:152
  258.7 1.2 gather_fusion.1
  260.2 1.4 multiply_reduce_fusion
  261.5 7.4 %all-gather.9.cloned.1.call-done = bf16[512,1024]{0,1:T(8,128)(2,1)} async-done(((bf16[512,256]{0,1:T(8,128)(2,1)}), bf16[512,1024]{0,1:T(8,128)(2,1)}) %all-gather.9.cloned.1.call-update) | async-done | bytes 1048592 | tf_op jit(solution)/shard_map/all_gather | solution.py:106
  268.9 3.1 %convolution_convert_fusion.1 = bf16[512,512]{1,0:T(8,128)(2,1)} fusion(bf16[512,1024]{0,1:T(8,128)(2,1)} %all-gather.9.cloned.1.call-done, bf16[1024,512]{1,0:T(8,128)(2,1)} %param.28), kind=kOutput, calls=%fused_computation.38 | convolution fusion | flops 537133056 | bytes 2621440 | tf_op jit(solution)/shard_map/dot_general | solution.py:105
  (141 shorter events, 24.3 us)
Async XLA Ops:
  7.2 62.1 %copy-start = (bf16[1,256,2048]{2,1,0:T(8,128)(2,1)S(1)}, bf16[1,256,2048]{2,1,0:T(8,128)(2,1)}, u32[]{:S(2)}) copy-start(bf16[1,256,2048]{2,1,0:T(8,128)(2,1)} %param.35) | copy-start | bytes 3145732
  7.2 59.8 %all-gather.11.cloned.1.call-start = ((), (), s32[]{:S(2)}) async-start(), calls=%async_computation.6 | async-start | bytes 1966080 | tf_op jit(solution)/shard_map/all_gather | solution.py:135
  15.8 21.5 %copy-start.6 = (f32[64]{0:T(128)S(1)}, f32[64]{0:T(128)}, u32[]{:S(2)}) copy-start(f32[64]{0:T(128)} %param.25) | copy-start | bytes 772
  15.8 23.7 %copy-start.8 = (f32[2048]{0:T(1024)S(1)}, f32[2048]{0:T(1024)}, u32[]{:S(2)}) copy-start(f32[2048]{0:T(1024)} %param.20) | copy-start | bytes 24580
  37.2 79.4 %all-gather.5.cloned.1.call-start = ((), (), s32[]{:S(2)}) async-start(), calls=%async_computation.3 | async-start | bytes 4866048 | tf_op jit(solution)/shard_map/all_gather | solution.py:61
  37.4 5.2 %copy-start.3 = (f32[512,4]{0,1:T(4,128)S(1)}, f32[512,4]{0,1:T(4,128)}, u32[]{:S(2)}) copy-start(f32[512,4]{0,1:T(4,128)} %param.26) | copy-start | bytes 24580
  39.5 4.1 %copy-start.1 = (bf16[512,2048]{1,0:T(8,128)(2,1)S(1)}, bf16[512,2048]{1,0:T(8,128)(2,1)}, u32[]{:S(2)}) copy-start(bf16[512,2048]{1,0:T(8,128)(2,1)} %param.19) | copy-start | bytes 6291460
  42.5 3.9 %copy-start.5 = (f32[256]{0:T(256)S(1)}, f32[256]{0:T(256)}, u32[]{:S(2)}) copy-start(f32[256]{0:T(256)} %param.27) | copy-start | bytes 3076
  43.5 102.7 %all-gather.7.cloned.1.call-start = ((), (), s32[]{:S(2)}) async-start(), calls=%async_computation.4 | async-start | bytes 2359296 | tf_op jit(solution)/shard_map/all_gather | solution.py:65
  46.2 2.4 copy-start.7
  46.3 196.5 %reduce-scatter.2.cloned.1.call-start = ((), (), s32[]{:S(2)}) async-start(), calls=%async_computation.7 | async-start | bytes 1966080 | tf_op jit(solution)/shard_map/reduce_scatter | solution.py:148
  74.0 72.2 %copy-start.2 = (f32[4,512,64]{1,2,0:T(8,128)S(1)}, f32[4,512,64]{1,2,0:T(8,128)}, u32[]{:S(2)}) copy-start(f32[4,512,64]{1,2,0:T(8,128)} %custom-call.2) | copy-start | bytes 1572868
  74.0 194.9 %all-gather.9.cloned.1.call-start = ((), (), s32[]{:S(2)}) async-start(), calls=%async_computation.5 | async-start | bytes 1310720 | tf_op jit(solution)/shard_map/all_gather | solution.py:106
  116.6 29.6 %slice-start = ((f32[4096,260]{0,1:T(8,128)}), f32[4096,4]{0,1:T(4,128)S(1)}, s32[]{:S(2)}) async-start(f32[4096,260]{0,1:T(8,128)} %all-gather.5.cloned.1.call-done), calls=%async_computation.8 | async-start | bytes 131072 | tf_op jit(solution)/shard_map/split | solution.py:60
  146.2 100.0 %copy-start.4 = (f32[128,2]{0,1:T(2,128)S(1)}, f32[128,2]{0,1:T(2,128)}, u32[]{:S(2)}) copy-start(f32[128,2]{0,1:T(2,128)} %param.32) | copy-start | bytes 3076
  242.8 15.9 %all-to-all-start.1 = ((bf16[8,48,512]{2,1,0:T(8,128)(2,1)}), bf16[8,48,512]{2,1,0:T(8,128)(2,1)S(1)}, u32[]{:S(2)}, u32[]{:S(2)}) async-start(bf16[8,48,512]{2,1,0:T(8,128)(2,1)} %bitcast.137), calls=%async_computation.2 | async-start | bytes 786432 | tf_op jit(solution)/shard_map/all_to_all | solution.py:152
Sparse Core Ops, SparseCore 0:
  37.3 29.6 all-gather.10
  68.6 47.9 all-gather.4
  118.2 27.9 all-gather.6
  149.0 30.5 reduce-scatter.1
  242.8 26.0 all-gather.8
